TPU v7x, 32 devices: a whole 2x2x4 slice. The times are simulated.
32 devices in a mesh: ep: 8 (over z, core), tp: 4 (over y, x).
Axes of the slice: x: 2, y: 2, z: 4, core: 2. Of those that a mesh axis runs over, the one named last changes fastest.
Arguments:
- queries: bfloat16 [2048, 2048], P('ep', 'tp'), may hold values from -6 to 6
- keys: bfloat16 [2048, 2048], P('ep', 'tp'), may hold values from -6 to 6
- values: bfloat16 [2048, 2048], P('ep', 'tp'), may hold values from -6 to 6
- gates: bfloat16 [2048, 2048], P('ep', 'tp'), may hold values from -6 to 6
- log_decay: float32 [2048, 16], P('ep', 'tp'), may hold values from -2 to 0
- out_weight: bfloat16 [2048, 2048], P(None, 'tp'), may hold values from -0.125 to 0.125
- moe_rows: bfloat16 [2048, 2048], P('ep'), may hold values from -140 to 140
- moe_gain: bfloat16 [2048], replicated, may hold values from 0.099609375 to 1.8984375
- routes: int32 [2048, 2], P('ep'), may hold values from 0 to 7, as said below
- route_weights: float32 [2048, 2], P('ep'), may hold values from 0.1 to 1
- gate_proj: bfloat16 [8, 2048, 4096], P('ep', None, 'tp'), may hold values from -0.125 to 0.125
- up_proj: bfloat16 [8, 2048, 4096], P('ep', None, 'tp'), may hold values from -0.125 to 0.125
- down_proj: bfloat16 [8, 4096, 2048], P('ep', None, 'tp'), may hold values from -0.09375 to 0.09375
Outputs:
- mixer_out: bfloat16 [2048, 2048], P('ep', 'tp')
- moe_out: bfloat16 [2048, 2048], P('ep', 'tp')
Inputs may be any that keep to these rules, and one draw needn't show every extreme that they name: `routes`: each row names two different experts of one group of 8 consecutive experts; in each aligned block of 256 rows every expert is named by exactly 64 rows.
All inputs are finite; a program needn't handle non-finite values.
Results may differ from a plain program's by a relative error of at most 0.011.
Values may be sent and summed in bfloat16 or wider, within the bound.
A program may use at most 64 MiB of HBM per device.

v0:
```python
import jax
import jax.numpy as jnp
from jax import lax
from jax.sharding import PartitionSpec as P

BLOCK = 128


def carried_in(value, axis, join, neutral):
    count, mine = (lax.axis_size(axis), lax.axis_index(axis))
    pieces = jax.tree.map(lambda part: lax.all_gather(part, axis), value)
    total = jax.tree.map(
        lambda part, zero: jnp.full_like(part, 0) + jnp.asarray(zero, part.dtype), value, neutral
    )

    def turn(position, total):
        longer = join(total, jax.tree.map(lambda part: part[position], pieces))
        return jax.tree.map(lambda new, old: jnp.where(position < mine, new, old), longer, total)

    return lax.fori_loop(0, count - 1, turn, total)


def rotate(source, positions, heads_here, factor):
    row_count, feat_width = source.shape
    head_dim = feat_width // heads_here
    half_dim = head_dim // 2
    values_f = source.astype(jnp.float32).reshape(row_count, heads_here, head_dim)
    inverse = 10000.0 ** (-jnp.arange(half_dim, dtype=jnp.float32) / half_dim)
    angles = positions[:, None] * inverse[None, :]
    cosine = jnp.cos(angles)[:, None, :]
    sine_part = jnp.sin(angles)[:, None, :]
    first_half = values_f[..., :half_dim]
    second_half = values_f[..., half_dim:]
    turned = jnp.concatenate(
        [
            first_half * cosine - second_half * sine_part,
            first_half * sine_part + second_half * cosine,
        ],
        axis=-1,
    )
    return (turned * factor).astype(jnp.bfloat16).reshape(row_count, feat_width)


def chain_states(earlier, later):
    return (earlier[0] * later[0], later[0][:, None, None] * earlier[1] + later[1])


def retention_half(queries, keys, values, gates, log_decay, out_weight):
    row_count, feat_width = queries.shape
    heads_here = log_decay.shape[1]
    head_dim = feat_width // heads_here
    block_count = row_count // BLOCK
    positions = (lax.axis_index("ep") * row_count + jnp.arange(row_count, dtype=jnp.int32)).astype(
        jnp.float32
    )
    rot_q = rotate(queries, positions, heads_here, 1.0)
    rot_k = rotate(keys, positions, heads_here, head_dim ** (-0.5))
    block_shape = (block_count, BLOCK, heads_here, head_dim)
    q_blocks = rot_q.reshape(block_shape)
    k_blocks = rot_k.reshape(block_shape)
    v_blocks = values.reshape(block_shape)
    cumulative = jnp.cumsum(log_decay.reshape(block_count, BLOCK, heads_here), axis=1)
    across = jnp.swapaxes(cumulative, 1, 2)
    spread = across[..., :, None] - across[..., None, :]
    causal = jnp.arange(BLOCK)[:, None] >= jnp.arange(BLOCK)[None, :]
    weights = jnp.where(causal, jnp.exp(jnp.where(causal, spread, 0.0)), 0.0)
    scores = jnp.einsum("nihd,njhd->nhij", q_blocks, k_blocks, preferred_element_type=jnp.float32)
    rounded = (scores * weights).astype(jnp.bfloat16)
    inside = jnp.einsum("nhij,njhd->nihd", rounded, v_blocks, preferred_element_type=jnp.float32)
    ending = cumulative[:, -1, :]
    k_scaled = k_blocks.astype(jnp.float32) * jnp.exp(ending[:, None, :] - cumulative)[..., None]
    updates = jnp.einsum(
        "njhd,njhe->nhde", k_scaled, v_blocks.astype(jnp.float32), precision=lax.Precision.HIGHEST
    )

    def advance(carry_state, member):
        return (jnp.exp(member[0])[:, None, None] * carry_state + member[1], carry_state)

    zero_state = jnp.zeros((heads_here, head_dim, head_dim), jnp.float32)
    local_end, before = lax.scan(advance, zero_state, (ending, updates))
    device_decay = jnp.exp(jnp.sum(ending, axis=0))
    incoming = carried_in(
        (device_decay, local_end), "ep", chain_states, (jnp.ones_like(device_decay), zero_state)
    )
    leading = jnp.cumsum(ending, axis=0) - ending
    entering = before + jnp.exp(leading)[:, :, None, None] * incoming[1][None]
    carried = (
        jnp.einsum(
            "nihd,nhde->nihe",
            q_blocks.astype(jnp.float32),
            entering,
            precision=lax.Precision.HIGHEST,
        )
        * jnp.exp(cumulative)[..., None]
    )
    retained = (inside + carried).reshape(row_count, heads_here, head_dim)
    gate_f = gates.astype(jnp.float32).reshape(row_count, heads_here, head_dim)
    scaled = retained * lax.rsqrt(jnp.mean(retained * retained, axis=-1, keepdims=True) + 1e-05)
    head_out = (scaled * jax.nn.silu(gate_f)).astype(jnp.bfloat16).reshape(row_count, feat_width)
    projected = jnp.dot(
        lax.all_gather(head_out, "tp", axis=1, tiled=True),
        out_weight,
        preferred_element_type=jnp.float32,
    )
    return projected.astype(jnp.bfloat16)


def expert_half(moe_rows, moe_gain, routes, route_weights, gate_proj, up_proj, down_proj):
    row_count, feat_width = moe_rows.shape
    experts = lax.axis_size("ep")
    capacity = 2 * row_count // experts
    as_float = moe_rows.astype(jnp.float32)
    normed = (
        as_float
        * lax.rsqrt(jnp.mean(as_float * as_float, axis=-1, keepdims=True) + 1e-06)
        * moe_gain.astype(jnp.float32)
    ).astype(jnp.bfloat16)
    flat_ids = routes.reshape(-1)
    onehot = (flat_ids[:, None] == jnp.arange(experts, dtype=jnp.int32)[None, :]).astype(jnp.int32)
    slot_rank = jnp.sum((jnp.cumsum(onehot, axis=0) - onehot) * onehot, axis=1)
    target = flat_ids * capacity + slot_rank
    source_row = (
        jnp.zeros((experts * capacity,), jnp.int32)
        .at[target]
        .set(jnp.arange(2 * row_count, dtype=jnp.int32) // 2)
    )
    outgoing = normed[source_row].reshape(experts, capacity, feat_width)
    w_gate = gate_proj[0]
    w_up = up_proj[0]
    w_down = down_proj[0]
    arrived_rows = lax.all_to_all(outgoing, "ep", split_axis=0, concat_axis=0, tiled=True)
    gate_part = jnp.einsum("scd,df->scf", arrived_rows, w_gate, preferred_element_type=jnp.float32)
    up_part = jnp.einsum("scd,df->scf", arrived_rows, w_up, preferred_element_type=jnp.float32)
    hidden = (jax.nn.silu(gate_part) * up_part).astype(jnp.bfloat16)
    expert_out = jnp.einsum(
        "scf,fd->scd",
        lax.all_gather(hidden, "tp", axis=2, tiled=True),
        w_down,
        preferred_element_type=jnp.float32,
    ).astype(jnp.bfloat16)
    returned = lax.all_to_all(expert_out, "ep", split_axis=0, concat_axis=0, tiled=True)
    picked = returned.reshape(experts * capacity, -1)[target].reshape(row_count, 2, -1)
    return jnp.sum(picked.astype(jnp.float32) * route_weights[:, :, None], axis=1).astype(
        jnp.bfloat16
    )


def on_device(
    queries,
    keys,
    values,
    gates,
    log_decay,
    out_weight,
    moe_rows,
    moe_gain,
    routes,
    route_weights,
    gate_proj,
    up_proj,
    down_proj,
):
    mixer_out = retention_half(queries, keys, values, gates, log_decay, out_weight)
    moe_out = expert_half(moe_rows, moe_gain, routes, route_weights, gate_proj, up_proj, down_proj)
    return (mixer_out, moe_out)


def solution(mesh):
    placed = (
        P("ep", "tp"),
        P("ep", "tp"),
        P("ep", "tp"),
        P("ep", "tp"),
        P("ep", "tp"),
        P(None, "tp"),
        P("ep", None),
        P(),
        P("ep", None),
        P("ep", None),
        P("ep", None, "tp"),
        P("ep", None, "tp"),
        P("ep", None, "tp"),
    )
    return jax.shard_map(
        on_device,
        mesh=mesh,
        in_specs=placed,
        out_specs=(P("ep", "tp"), P("ep", "tp")),
        check_vma=False,
    )
```

profile of v0, /device:TPU:0, one launch (start us, length us, event | category | flops | bytes accessed | tf_op | source)
XLA Modules:
  0.0 199.5 jit_solution(13536535929649242897)
XLA Ops:
  7.2 1.0 copy.86
  9.1 1.1 reduce-window.6
  10.9 2.4 %scatter_custom_fusion = s32[512]{0:T(512)S(1)} fusion(s32[512]{0:T(512)S(1)} %bitcast.110, s32[512]{0:T(512)S(1)} %add_select_fusion, s32[]{:T(128)} %copy.125), kind=kCustom, calls=%fused_computation.90 | custom fusion | bytes 2052 | tf_op jit(solution)/shard_map/scatter | solution.py:125
  13.4 0.7 convert_element_type.72
  14.1 1.5 fusion.9
  15.6 1.5 fusion.11
  17.2 3.3 %gather_fusion = bf16[512,2048]{1,0:T(8,128)(2,1)} fusion(bf16[256,2048]{1,0:T(8,128)(2,1)S(1)} %fusion.11, s32[1024]{0:T(1024)S(1)} %pad_clamp_fusion.1), kind=kCustom, calls=%fused_computation | custom fusion | bytes 4196352 | tf_op jit(solution)/shard_map/gather | solution.py:127
  20.5 6.5 %all-to-all-start = ((bf16[8,64,2048]{2,1,0:T(8,128)(2,1)}), bf16[8,64,2048]{2,1,0:T(8,128)(2,1)}, u32[]{:S(2)}, u32[]{:S(2)}) async-start(bf16[8,64,2048]{2,1,0:T(8,128)(2,1)} %bitcast.100), calls=%async_computation | async-start | bytes 4194304 | tf_op jit(solution)/shard_map/all_to_all | solution.py:131
  27.2 1.1 copy.93
  28.6 1.0 subtract_convert_fusion
  29.6 1.1 concatenate.20
  30.9 1.8 concatenate.21
  32.7 1.1 copy.73
  33.8 0.8 copy.91
  34.6 1.1 reduce_window_sum.37
  35.7 0.7 fusion.56
  36.5 1.0 copy.78
  37.5 1.7 reshape.218
  40.1 1.7 fusion.27
  41.8 1.7 while.29
  41.8 0.7 bitcast_dynamic-update-slice_fusion.3
  42.7 0.7 bitcast_dynamic-update-slice_fusion.3
  43.5 0.7 copy-done.1
  44.3 48.7 %all-to-all-done = bf16[8,64,2048]{2,1,0:T(8,128)(2,1)} async-done(((bf16[8,64,2048]{2,1,0:T(8,128)(2,1)}), bf16[8,64,2048]{2,1,0:T(8,128)(2,1)}, u32[]{:S(2)}, u32[]{:S(2)}) %all-to-all-start) | async-done | bytes 2097184 | tf_op jit(solution)/shard_map/all_to_all | solution.py:131
  92.9 5.3 %fusion.7 = f32[8,64,1024]{2,1,0:T(8,128)S(1)} fusion(bf16[8,64,2048]{2,1,0:T(8,128)(2,1)} %all-to-all-done, bf16[1,2048,1024]{2,1,0:T(8,128)(2,1)} %param.27), kind=kOutput, calls=%fused_computation.15 | convolution fusion | flops 2147483648 | bytes 8388608 | tf_op jit(solution)/shard_map/scd,df->scf/dot_general | solution.py:132
  98.3 5.2 %multiply_convert_fusion = bf16[8,64,1024]{2,1,0:T(8,128)(2,1)} fusion(f32[8,64,1024]{2,1,0:T(8,128)S(1)} %fusion.7, bf16[8,64,2048]{2,1,0:T(8,128)(2,1)} %all-to-all-done, bf16[1,2048,1024]{2,1,0:T(8,128)(2,1)S(1)} %copy-done.11), kind=kOutput, calls=%fused_computation.22 | convolution fusion | flops 2150629376 | bytes 9437184 | tf_op jit(solution)/shard_map/scd,df->scf/dot_general | solution.py:133
  105.0 14.7 %all-reduce = f32[32]{0:T(128)S(1)} all-reduce(f32[32]{0:T(128)S(1)} %exponential_dynamic-update-slice_fusion), channel_id=2, replica_groups=mesh['ep'=8,'tp'=4] {'ep'}, use_global_device_ids=true, to_apply=%add | all-reduce | flops 32 | bytes 256
  121.2 12.4 %while.30 = (s32[]{:T(128)}, f32[4,128,128]{2,1,0:T(8,128)S(1)}, s32[]{:T(128)}, f32[8,4]{1,0:T(8,128)}, f32[8,4,128,128]{3,2,1,0:T(8,128)}) while((s32[]{:T(128)}, f32[4,128,128]{2,1,0:T(8,128)S(1)}, s32[]{:T(128)}, f32[8,4]{1,0:T(8,128)}, f32[8,4,128,128]{3,2,1,0:T(8,128)}) %tuple.79), condition=%wide.region_6.7_spmd.clone.clone, body=%wide.region_5.6_spmd.clone.sunk.clone | while | flops 262148 | bytes 786569 | solution.py:20
  121.2 0.7 dynamic-slice_bitcast_fusion.3
  121.9 1.0 fusion.68
  123.7 1.0 fusion.68
  125.4 1.0 fusion.68
  127.2 1.0 fusion.68
  128.9 1.0 fusion.68
  130.7 1.1 fusion.68
  132.5 1.0 fusion.68
  133.6 2.5 %fusion.18 = f32[2,128,4,128]{1,3,2,0:T(8,128)} fusion(f32[2,4,128,128]{3,2,1,0:T(8,128)} %get-tuple-element.124, f32[2,128,4]{1,2,0:T(4,128)S(1)} %copy.82, f32[4,128,128]{2,1,0:T(8,128)S(1)} %get-tuple-element.126, f32[2,4]{1,0:T(2,128)S(1)} %subtract_exponential_fusion.1, bf16[2,128,4,64]{3,1,2,0:T(8,128)(2,1)S(1)} %copy.69, ...), kind=kOutput, calls=%fused_computation.28 | convolution fusion | flops 202244096 | bytes 1576992 | tf_op jit(solution)/shard_map/nihd,nhde->nihe/dot_general | solution.py:88
  136.1 2.4 %multiply_reduce_fusion.1 = (f32[2,128,4]{1,2,0:T(4,128)S(1)}, f32[2,128,4,128]{1,3,2,0:T(8,128)}) fusion(f32[2,128,4,128]{1,3,2,0:T(8,128)} %fusion.18, bf16[2,128,4,128]{3,2,1,0:T(4,128)(2,1)S(1)} %copy-done.4, bf16[2,128,4,128]{3,1,2,0:T(8,128)(2,1)S(1)} %copy-done.3, f32[2,4,128]{2,1,0:T(4,128)S(1)} %copy.75, ...), kind=kOutput, calls=%fused_computation.41 | convolution fusion | flops 68680704 | bytes 1859584 | tf_op jit(solution)/shard_map/nhij,njhd->nihd/dot_general | solution.py:69
  138.7 1.3 copy.83
  140.3 1.8 fusion.34
  142.2 13.0 %all-gather.8.cloned.1.call-done = bf16[8,64,4096]{2,1,0:T(8,128)(2,1)} async-done(((bf16[8,64,1024]{2,1,0:T(8,128)(2,1)}), bf16[8,64,4096]{2,1,0:T(8,128)(2,1)}) %all-gather.8.cloned.1.call-update) | async-done | bytes 4194320 | tf_op jit(solution)/shard_map/all_gather | solution.py:137
  155.2 6.6 %fusion.14 = bf16[8,64,512]{2,1,0:T(8,128)(2,1)} fusion(bf16[8,64,4096]{2,1,0:T(8,128)(2,1)} %all-gather.8.cloned.1.call-done, bf16[1,4096,512]{2,1,0:T(8,128)(2,1)} %param.29), kind=kOutput, calls=%fused_computation.23 | convolution fusion | flops 2147745792 | bytes 8912896 | tf_op jit(solution)/shard_map/scf,fd->scd/dot_general | solution.py:135
  161.8 4.6 %all-to-all-start.1 = ((bf16[8,64,512]{2,1,0:T(8,128)(2,1)}), bf16[8,64,512]{2,1,0:T(8,128)(2,1)S(1)}, u32[]{:S(2)}, u32[]{:S(2)}) async-start(bf16[8,64,512]{2,1,0:T(8,128)(2,1)} %fusion.14), calls=%async_computation.1 | async-start | bytes 1048576 | tf_op jit(solution)/shard_map/all_to_all | solution.py:141
  166.5 17.4 %all-gather.6.cloned.1.call-done = bf16[256,2048]{1,0:T(8,128)(2,1)} async-done(((bf16[256,512]{1,0:T(8,128)(2,1)}), bf16[256,2048]{1,0:T(8,128)(2,1)}) %all-gather.6.cloned.1.call-update) | async-done | bytes 1048592 | tf_op jit(solution)/shard_map/all_gather | solution.py:101
  184.0 2.6 %convolution_convert_fusion = bf16[256,512]{1,0:T(8,128)(2,1)} fusion(bf16[256,2048]{1,0:T(8,128)(2,1)} %all-gather.6.cloned.1.call-done, bf16[2048,512]{1,0:T(8,128)(2,1)S(1)} %copy-done), kind=kOutput, calls=%fused_computation.29 | convolution fusion | flops 537001984 | bytes 3407872 | tf_op jit(solution)/shard_map/dot_general | solution.py:100
  186.6 2.6 %gather_fusion.1 = bf16[512,512]{1,0:T(8,128)(2,1)} fusion(bf16[512,512]{1,0:T(8,128)(2,1)S(1)} %bitcast.99, s32[1024]{0:T(1024)S(1)} %pad_clamp_fusion), kind=kCustom, calls=%fused_computation.1 | custom fusion | bytes 1050624 | tf_op jit(solution)/shard_map/gather | solution.py:142
  189.2 1.7 reshape.227
  190.9 2.1 %multiply_reduce_fusion = bf16[256,512]{1,0:T(8,128)(2,1)} fusion(f32[256,2,512]{2,1,0:T(2,128)S(1)} %reshape.227, f32[256,2]{1,0:T(8,128)S(1)} %copy.88), kind=kLoop, calls=%fused_computation.31 | loop fusion | flops 393216 | bytes 1312768 | tf_op jit(solution)/shard_map/reduce_sum | solution.py:143
  (86 shorter events, 10.5 us)
Async XLA Ops:
  7.2 176.8 %copy-start = (bf16[2048,512]{1,0:T(8,128)(2,1)S(1)}, bf16[2048,512]{1,0:T(8,128)(2,1)}, u32[]{:S(2)}) copy-start(bf16[2048,512]{1,0:T(8,128)(2,1)} %param.22) | copy-start | bytes 6291460
  20.5 6.6 %copy-start.8 = (bf16[256,512]{1,0:T(8,128)(2,1)S(1)}, bf16[256,512]{1,0:T(8,128)(2,1)}, u32[]{:S(2)}) copy-start(bf16[256,512]{1,0:T(8,128)(2,1)} %param.17) | copy-start | bytes 786436
  20.5 72.5 %all-to-all-start = ((bf16[8,64,2048]{2,1,0:T(8,128)(2,1)}), bf16[8,64,2048]{2,1,0:T(8,128)(2,1)}, u32[]{:S(2)}, u32[]{:S(2)}) async-start(bf16[8,64,2048]{2,1,0:T(8,128)(2,1)} %bitcast.100), calls=%async_computation | async-start | bytes 4194304 | tf_op jit(solution)/shard_map/all_to_all | solution.py:131
  26.9 94.2 %all-gather.10.cloned.1.call-start = ((), (), s32[]{:S(2)}) async-start(), calls=%async_computation.4 | async-start | bytes 2359296 | tf_op jit(solution)/shard_map/all_gather | solution.py:11
  28.6 5.2 %copy-start.9 = (f32[256,4]{0,1:T(4,128)S(1)}, f32[256,4]{0,1:T(4,128)}, u32[]{:S(2)}) copy-start(f32[256,4]{0,1:T(4,128)} %param.21) | copy-start | bytes 12292
  39.4 0.7 copy-start.2
  43.5 0.7 copy-start.1
  44.2 110.9 %all-gather.8.cloned.1.call-start = ((), (), s32[]{:S(2)}) async-start(), calls=%async_computation.3 | async-start | bytes 5242880 | tf_op jit(solution)/shard_map/all_gather | solution.py:137
  92.9 5.3 %copy-start.11 = (bf16[1,2048,1024]{2,1,0:T(8,128)(2,1)S(1)}, bf16[1,2048,1024]{2,1,0:T(8,128)(2,1)}, u32[]{:S(2)}) copy-start(bf16[1,2048,1024]{2,1,0:T(8,128)(2,1)} %param.28) | copy-start | bytes 12582916
  98.2 5.4 %copy-start.12 = (u32[32]{0:T(128)S(1)}, u32[32]{0:T(128)}, u32[]{:S(2)}) copy-start(u32[32]{0:T(128)} %constant.105) | copy-start | bytes 388
  98.3 22.2 %copy-start.7 = (bf16[256,4,64]{0,2,1:T(8,128)(2,1)S(1)}, bf16[256,4,64]{0,2,1:T(8,128)(2,1)}, u32[]{:S(2)}) copy-start(bf16[256,4,64]{0,2,1:T(8,128)(2,1)} %get-tuple-element.183) | copy-start | bytes 393220
  98.3 22.4 %copy-start.6 = (bf16[256,4,64]{0,2,1:T(8,128)(2,1)S(1)}, bf16[256,4,64]{0,2,1:T(8,128)(2,1)}, u32[]{:S(2)}) copy-start(bf16[256,4,64]{0,2,1:T(8,128)(2,1)} %get-tuple-element.184) | copy-start | bytes 393220
  103.5 17.5 %copy-start.5 = (f32[2,128,4]{2,1,0:T(8,128)S(1)}, f32[2,128,4]{2,1,0:T(8,128)}, u32[]{:S(2)}) copy-start(f32[2,128,4]{2,1,0:T(8,128)} %get-tuple-element.191) | copy-start | bytes 12292
  103.5 80.5 %all-gather.6.cloned.1.call-start = ((), (), s32[]{:S(2)}) async-start(), calls=%async_computation.2 | async-start | bytes 1310720 | tf_op jit(solution)/shard_map/all_gather | solution.py:101
  121.2 14.9 %copy-start.3 = (bf16[2,128,4,128]{3,1,2,0:T(8,128)(2,1)S(1)}, bf16[2,128,4,128]{3,1,2,0:T(8,128)(2,1)}, u32[]{:S(2)}) copy-start(bf16[2,128,4,128]{3,1,2,0:T(8,128)(2,1)} %copy-done.2) | copy-start | bytes 786436
  121.2 14.9 %copy-start.4 = (bf16[2,128,4,128]{3,2,1,0:T(4,128)(2,1)S(1)}, bf16[2,128,4,128]{3,2,1,0:T(4,128)(2,1)}, u32[]{:S(2)}) copy-start(bf16[2,128,4,128]{3,2,1,0:T(4,128)(2,1)} %reshape.218) | copy-start | bytes 786436
  142.2 24.2 %copy-start.10 = (f32[256,2]{0,1:T(2,128)S(1)}, f32[256,2]{0,1:T(2,128)}, u32[]{:S(2)}) copy-start(f32[256,2]{0,1:T(2,128)} %param.26) | copy-start | bytes 6148
  161.8 24.8 %all-to-all-start.1 = ((bf16[8,64,512]{2,1,0:T(8,128)(2,1)}), bf16[8,64,512]{2,1,0:T(8,128)(2,1)S(1)}, u32[]{:S(2)}, u32[]{:S(2)}) async-start(bf16[8,64,512]{2,1,0:T(8,128)(2,1)} %fusion.14), calls=%async_computation.1 | async-start | bytes 1048576 | tf_op jit(solution)/shard_map/all_to_all | solution.py:141
Sparse Core Ops, SparseCore 0:
  44.3 48.1 all-gather.9
  103.6 51.5 all-gather.7
  157.6 26.3 all-gather.5
where the time goes:
time: 201 us; the launch traced here: 200 us
  waiting for transfers between devices  79.1 us (39%)
  local copies, waits for them, and re-layouts  30.9 us (15%)
  matrix products  26.4 us (13%)
  other arithmetic  22.1 us (11%)
  between operations  14.8 us (7%)
  blocking collectives  14.7 us (7%)
  starting transfers between devices  11.2 us (6%)
    all_to_all x1, waiting for transfers between devices, expert_half(): lax.all_to_all(outgoing, 'ep', split_axis=0, concat_axis=0, tiled=True)  48.7 us
    all_gather x1, waiting for transfers between devices, retention_half(): lax.all_gather(head_out, 'tp', axis=1, tiled=True)  17.4 us
    unnamed x1, blocking collectives  14.7 us
    all_gather x1, waiting for transfers between devices, expert_half(): lax.all_gather(hidden, 'tp', axis=2, tiled=True)  13 us
    select_n x7, other arithmetic, turn(): jnp.where(position < mine, new, old)  7.41 us
    dot_general x1, matrix products, expert_half(): jnp.einsum('scf,fd->scd', lax.all_gather(hidden, 'tp', axis=2, tiled=True...  6.6 us
    all_to_all x1, starting transfers between devices, expert_half(): lax.all_to_all(outgoing, 'ep', split_axis=0, concat_axis=0, tiled=True)  6.49 us
    dot_general x1, matrix products, expert_half(): jnp.einsum('scd,df->scf', arrived_rows, w_gate, preferred_element_type=jn...  5.3 us
  transfers between devices with their start and end apart: 5, of which 3 were waited for; matrix products, arithmetic and copies ran while one was open for 29% of the time, Pallas kernels for 0%

commit v1 on v0

--- a/solution.py
+++ b/solution.py
@@ -4,6 +4,19 @@
 from jax.sharding import PartitionSpec as P
 
 BLOCK = 128
+
+
+def ring_gather(shard, axis, dim):
+    ways = lax.axis_size(axis)
+    up = [(d, (d + 1) % ways) for d in range(ways)]
+    down = [(d, (d - 1) % ways) for d in range(ways)]
+    earlier, later = ([shard], [shard])
+    for _ in range(ways // 2):
+        earlier.append(lax.ppermute(earlier[-1], axis, up))
+    for _ in range((ways - 1) // 2):
+        later.append(lax.ppermute(later[-1], axis, down))
+    line = jnp.concatenate([*earlier[::-1], *later[1:]], axis=dim)
+    return jnp.roll(line, (lax.axis_index(axis) - ways // 2) * shard.shape[dim], axis=dim)
 
 
 def carried_in(value, axis, join, neutral):
@@ -133,10 +146,7 @@
     up_part = jnp.einsum("scd,df->scf", arrived_rows, w_up, preferred_element_type=jnp.float32)
     hidden = (jax.nn.silu(gate_part) * up_part).astype(jnp.bfloat16)
     expert_out = jnp.einsum(
-        "scf,fd->scd",
-        lax.all_gather(hidden, "tp", axis=2, tiled=True),
-        w_down,
-        preferred_element_type=jnp.float32,
+        "scf,fd->scd", ring_gather(hidden, "tp", 2), w_down, preferred_element_type=jnp.float32
     ).astype(jnp.bfloat16)
     returned = lax.all_to_all(expert_out, "ep", split_axis=0, concat_axis=0, tiled=True)
     picked = returned.reshape(experts * capacity, -1)[target].reshape(row_count, 2, -1)

time: 201 us -> 233 us (1.16)
  local copies, waits for them, and re-layouts: 30.9 us -> 48.9 us
  waiting for transfers between devices: 79.1 us -> 92.8 us
  matrix products: 26.4 us -> 22.4 us
  starting transfers between devices: 11.2 us -> 13.6 us
    ppermute x0 -> x3, waiting for transfers between devices: none -> 31.8 us  [the longest x2 31.8 us: ring_gather(): earlier.append(lax.ppermute(earlier[-1], axis, up))]
    all_gather x1, waiting for transfers between devices: 17.4 us -> 0.02 us  [retention_half(): lax.all_gather(head_out, 'tp', axis=1, tiled=True)]
    all_gather x1 -> x0, waiting for transfers between devices: 13 us -> none  [expert_half(): lax.all_gather(hidden, 'tp', axis=2, tiled=True)]
    all_to_all x1, waiting for transfers between devices: 0.01 us -> 12.4 us  [expert_half(): lax.all_to_all(expert_out, 'ep', split_axis=0, concat_axis=0, tiled=True)]
    unnamed x31 -> x32, local copies, waits for them, and re-layouts: 3.29 us -> 12 us
    concatenate x8, local copies, waits for them, and re-layouts: 4.67 us -> 10.9 us  [rotate(): jnp.concatenate([first_half * cosine - second_half * sine_part, first_hal...]
    ppermute x0 -> x3, starting transfers between devices: none -> 3.57 us  [the longest x2 2.13 us: ring_gather(): earlier.append(lax.ppermute(earlier[-1], axis, up))]
    dot_general x1, matrix products: 6.6 us -> 3.15 us  [expert_half(): jnp.einsum('scf,fd->scd', ring_gather(hidden, 'tp', 2), w_down, preferred...]
  transfers between devices with their start and end apart: 5 -> 7, of which waited for: 3 -> 3; matrix products, arithmetic and copies ran while one was open for 29% -> 32% of each run, Pallas kernels for 0% -> 0%
where the time goes in v1:
time: 233 us; the launch traced here: 231 us
  waiting for transfers between devices  92.8 us (40%)
  local copies, waits for them, and re-layouts  48.9 us (21%)
  other arithmetic  24 us (10%)
  matrix products  22.4 us (10%)
  between operations  15 us (6%)
  blocking collectives  14.4 us (6%)
  starting transfers between devices  13.6 us (6%)
    all_to_all x1, waiting for transfers between devices, expert_half(): lax.all_to_all(outgoing, 'ep', split_axis=0, concat_axis=0, tiled=True)  48.6 us
    ppermute x2, waiting for transfers between devices, ring_gather(): earlier.append(lax.ppermute(earlier[-1], axis, up))  31.8 us
    unnamed x1, blocking collectives  14.4 us
    all_to_all x1, waiting for transfers between devices, expert_half(): lax.all_to_all(expert_out, 'ep', split_axis=0, concat_axis=0, tiled=True)  12.4 us
    unnamed x32, local copies, waits for them, and re-layouts  12 us
    concatenate x8, local copies, waits for them, and re-layouts, rotate(): jnp.concatenate([first_half * cosine - second_half * sine_part, first_hal...  10.9 us
    select_n x7, other arithmetic, turn(): jnp.where(position < mine, new, old)  7.34 us
    all_to_all x1, starting transfers between devices, expert_half(): lax.all_to_all(outgoing, 'ep', split_axis=0, concat_axis=0, tiled=True)  6.49 us
  transfers between devices with their start and end apart: 7, of which 3 were waited for; matrix products, arithmetic and copies ran while one was open for 32% of the time, Pallas kernels for 0%

profile of v1, /device:TPU:0, one launch (start us, length us, event | category | flops | bytes accessed | tf_op | source)
XLA Modules:
  0.0 231.3 jit_solution(5410723015288783803)
XLA Ops:
  9.1 1.1 reduce-window.6
  10.9 2.4 %scatter_custom_fusion = s32[512]{0:T(512)S(1)} fusion(s32[512]{0:T(512)S(1)} %bitcast.109, s32[512]{0:T(512)S(1)} %add_select_fusion, s32[]{:T(128)} %copy.132), kind=kCustom, calls=%fused_computation.99 | custom fusion | bytes 2052 | tf_op jit(solution)/shard_map/scatter | solution.py:138
  14.1 1.5 fusion.10
  15.6 1.5 fusion.12
  17.2 3.3 %gather_fusion = bf16[512,2048]{1,0:T(8,128)(2,1)} fusion(bf16[256,2048]{1,0:T(8,128)(2,1)S(1)} %fusion.12, s32[1024]{0:T(1024)S(1)} %pad_clamp_fusion.1), kind=kCustom, calls=%fused_computation | custom fusion | bytes 4196352 | tf_op jit(solution)/shard_map/gather | solution.py:140
  20.5 6.5 %all-to-all-start = ((bf16[8,64,2048]{2,1,0:T(8,128)(2,1)}), bf16[8,64,2048]{2,1,0:T(8,128)(2,1)}, u32[]{:S(2)}, u32[]{:S(2)}) async-start(bf16[8,64,2048]{2,1,0:T(8,128)(2,1)} %bitcast.99), calls=%async_computation | async-start | bytes 4194304 | tf_op jit(solution)/shard_map/all_to_all | solution.py:144
  27.2 1.1 copy.93
  29.6 1.1 concatenate.26
  30.9 1.8 concatenate.27
  32.7 1.1 copy.73
  34.7 1.1 reduce_window_sum.37
  37.5 1.7 reshape.218
  40.2 1.7 fusion.30
  41.9 1.7 while.29
  44.3 48.6 %all-to-all-done = bf16[8,64,2048]{2,1,0:T(8,128)(2,1)} async-done(((bf16[8,64,2048]{2,1,0:T(8,128)(2,1)}), bf16[8,64,2048]{2,1,0:T(8,128)(2,1)}, u32[]{:S(2)}, u32[]{:S(2)}) %all-to-all-start) | async-done | bytes 2097184 | tf_op jit(solution)/shard_map/all_to_all | solution.py:144
  93.0 5.3 %fusion.7 = f32[8,64,1024]{2,1,0:T(8,128)S(1)} fusion(bf16[8,64,2048]{2,1,0:T(8,128)(2,1)} %all-to-all-done, bf16[1,2048,1024]{2,1,0:T(8,128)(2,1)} %param.27), kind=kOutput, calls=%fused_computation.15 | convolution fusion | flops 2147483648 | bytes 8388608 | tf_op jit(solution)/shard_map/scd,df->scf/dot_general | solution.py:145
  98.3 4.1 %multiply_convert_fusion = bf16[8,64,1024]{2,1,0:T(8,128)(2,1)S(1)} fusion(f32[8,64,1024]{2,1,0:T(8,128)S(1)} %fusion.7, bf16[8,64,2048]{2,1,0:T(8,128)(2,1)} %all-to-all-done, bf16[1,2048,1024]{2,1,0:T(8,128)(2,1)S(1)} %copy-done.7), kind=kOutput, calls=%fused_computation.23 | convolution fusion | flops 2150629376 | bytes 9437184 | tf_op jit(solution)/shard_map/scd,df->scf/dot_general | solution.py:146
  102.4 1.5 collective-permute-start
  106.3 1.3 exponential_dynamic-update-slice_fusion
  107.7 14.4 %all-reduce = f32[32]{0:T(128)S(1)} all-reduce(f32[32]{0:T(128)} %exponential_dynamic-update-slice_fusion), channel_id=2, replica_groups=mesh['ep'=8,'tp'=4] {'ep'}, use_global_device_ids=true, to_apply=%add | all-reduce | flops 32 | bytes 256
  122.7 1.6 concatenate.23
  124.3 1.8 copy.68
  126.1 1.6 concatenate.24
  127.7 1.8 copy.69
  131.8 1.4 collective-permute-start.2
  133.8 12.2 %while.30 = (s32[]{:T(128)}, f32[4,128,128]{2,1,0:T(8,128)S(1)}, s32[]{:T(128)}, f32[8,4]{1,0:T(8,128)}, f32[8,4,128,128]{3,2,1,0:T(8,128)}) while((s32[]{:T(128)}, f32[4,128,128]{2,1,0:T(8,128)S(1)}, s32[]{:T(128)}, f32[8,4]{1,0:T(8,128)}, f32[8,4,128,128]{3,2,1,0:T(8,128)}) %tuple.77), condition=%wide.region_6.7_spmd.clone.clone, body=%wide.region_5.6_spmd.clone.sunk.clone | while | flops 262148 | bytes 786569 | solution.py:33
  134.5 1.0 fusion.71
  136.3 1.0 fusion.71
  138.0 1.0 fusion.71
  145.0 1.0 fusion.71
  146.1 2.7 %fusion.21 = f32[2,128,4,128]{1,3,2,0:T(8,128)} fusion(f32[2,4,128,128]{3,2,1,0:T(8,128)} %get-tuple-element.124, f32[2,128,4]{1,2,0:T(4,128)S(1)} %copy.82, f32[4,128,128]{2,1,0:T(8,128)S(1)} %get-tuple-element.126, f32[2,4]{1,0:T(2,128)S(1)} %subtract_exponential_fusion.1, bf16[2,128,4,64]{3,1,2,0:T(8,128)(2,1)} %copy.69, bf16[2,128,4,64]{3,1,2,0:T(8,128)(2,1)} %copy.68), kind=kOutput, calls=%fused_computation.29 | convolution fusion | flops 202244096 | bytes 1576992 | tf_op jit(solution)/shard_map/nihd,nhde->nihe/dot_general | solution.py:101
  148.8 2.8 %multiply_reduce_fusion.1 = (f32[2,128,4]{1,2,0:T(4,128)S(1)}, f32[2,128,4,128]{1,3,2,0:T(8,128)}) fusion(f32[2,128,4,128]{1,3,2,0:T(8,128)} %fusion.21, bf16[2,128,4,128]{3,2,1,0:T(4,128)(2,1)} %reshape.218, bf16[2,128,4,128]{3,1,2,0:T(8,128)(2,1)} %copy-done.2, f32[2,4,128]{2,1,0:T(4,128)S(1)} %copy.75, pred[128,128]{1,0:T(8,128)(4,1)} %iota_compare_fusion, ...), kind=kOutput, calls=%fused_computation.42 | convolution fusion | flops 68680704 | bytes 1859584 | tf_op jit(solution)/shard_map/nhij,njhd->nihd/dot_general | solution.py:82
  151.7 2.0 copy.83
  154.1 1.9 fusion.37
  156.1 31.8 %collective-permute-done.1 = bf16[8,64,1024]{2,1,0:T(8,128)(2,1)} collective-permute-done((bf16[8,64,1024]{2,1,0:T(8,128)(2,1)}, bf16[8,64,1024]{2,1,0:T(8,128)(2,1)}, u32[]{:S(2)}, u32[]{:S(2)}) %collective-permute-start.1) | collective-permute-done | bytes 1048608 | tf_op jit(solution)/shard_map/ppermute | solution.py:15
  187.8 1.3 constant_dynamic-update-slice_fusion.7
  189.1 1.3 constant_dynamic-update-slice_fusion.6
  190.6 1.3 constant_dynamic-update-slice_fusion.4
  191.9 1.5 constant_dynamic-update-slice_fusion.3
  193.4 1.4 constant_dynamic-update-slice_fusion.2
  194.9 1.3 constant_dynamic-update-slice_fusion
  196.2 3.1 %fusion.15 = bf16[8,64,512]{2,1,0:T(8,128)(2,1)} fusion(bf16[1,4096,512]{2,1,0:T(8,128)(2,1)S(1)} %copy-done.8, bf16[8,64,8192]{2,1,0:T(8,128)(2,1)S(1)} %constant_dynamic-update-slice_fusion, s32[]{:T(128)S(6)} %select_n.67), kind=kOutput, calls=%fused_computation.24 | convolution fusion | flops 2147745792 | bytes 8912900 | tf_op jit(solution)/shard_map/scf,fd->scd/dot_general | solution.py:148
  199.4 3.5 %all-to-all-start.1 = ((bf16[8,64,512]{2,1,0:T(8,128)(2,1)}), bf16[8,64,512]{2,1,0:T(8,128)(2,1)S(1)}, u32[]{:S(2)}, u32[]{:S(2)}) async-start(bf16[8,64,512]{2,1,0:T(8,128)(2,1)} %fusion.15), calls=%async_computation.1 | async-start | bytes 1048576 | tf_op jit(solution)/shard_map/all_to_all | solution.py:151
  203.1 2.6 %convolution_convert_fusion = bf16[256,512]{1,0:T(8,128)(2,1)} fusion(bf16[256,2048]{1,0:T(8,128)(2,1)} %all-gather.5.cloned.1.call-done, bf16[2048,512]{1,0:T(8,128)(2,1)S(1)} %copy-done), kind=kOutput, calls=%fused_computation.30 | convolution fusion | flops 537001984 | bytes 3407872 | tf_op jit(solution)/shard_map/dot_general | solution.py:113
  205.7 12.4 %all-to-all-done.1 = bf16[8,64,512]{2,1,0:T(8,128)(2,1)S(1)} async-done(((bf16[8,64,512]{2,1,0:T(8,128)(2,1)}), bf16[8,64,512]{2,1,0:T(8,128)(2,1)S(1)}, u32[]{:S(2)}, u32[]{:S(2)}) %all-to-all-start.1) | async-done | bytes 524320 | tf_op jit(solution)/shard_map/all_to_all | solution.py:151
  218.1 2.6 %gather_fusion.1 = bf16[512,512]{1,0:T(8,128)(2,1)} fusion(bf16[512,512]{1,0:T(8,128)(2,1)S(1)} %bitcast.98, s32[1024]{0:T(1024)S(1)} %pad_clamp_fusion), kind=kCustom, calls=%fused_computation.1 | custom fusion | bytes 1050624 | tf_op jit(solution)/shard_map/gather | solution.py:152
  220.7 1.7 reshape.227
  222.4 2.1 multiply_reduce_fusion
  (91 shorter events, 25.0 us)
Async XLA Ops:
  7.2 195.9 %copy-start = (bf16[2048,512]{1,0:T(8,128)(2,1)S(1)}, bf16[2048,512]{1,0:T(8,128)(2,1)}, u32[]{:S(2)}) copy-start(bf16[2048,512]{1,0:T(8,128)(2,1)} %param.22) | copy-start | bytes 6291460
  20.5 6.6 %copy-start.3 = (bf16[256,512]{1,0:T(8,128)(2,1)S(1)}, bf16[256,512]{1,0:T(8,128)(2,1)}, u32[]{:S(2)}) copy-start(bf16[256,512]{1,0:T(8,128)(2,1)} %param.17) | copy-start | bytes 786436
  20.5 72.5 %all-to-all-start = ((bf16[8,64,2048]{2,1,0:T(8,128)(2,1)}), bf16[8,64,2048]{2,1,0:T(8,128)(2,1)}, u32[]{:S(2)}, u32[]{:S(2)}) async-start(bf16[8,64,2048]{2,1,0:T(8,128)(2,1)} %bitcast.99), calls=%async_computation | async-start | bytes 4194304 | tf_op jit(solution)/shard_map/all_to_all | solution.py:144
  27.0 6.9 %copy-start.5 = (f32[256,4]{0,1:T(4,128)S(1)}, f32[256,4]{0,1:T(4,128)}, u32[]{:S(2)}) copy-start(f32[256,4]{0,1:T(4,128)} %param.21) | copy-start | bytes 12292
  27.0 106.9 %all-gather.7.cloned.1.call-start = ((), (), s32[]{:S(2)}) async-start(), calls=%async_computation.3 | async-start | bytes 2359296 | tf_op jit(solution)/shard_map/all_gather | solution.py:24
  39.4 0.7 copy-start.2
  43.6 0.7 copy-start.1
  44.3 158.8 %all-gather.5.cloned.1.call-start = ((), (), s32[]{:S(2)}) async-start(), calls=%async_computation.2 | async-start | bytes 1310720 | tf_op jit(solution)/shard_map/all_gather | solution.py:114
  93.0 5.3 %copy-start.7 = (bf16[1,2048,1024]{2,1,0:T(8,128)(2,1)S(1)}, bf16[1,2048,1024]{2,1,0:T(8,128)(2,1)}, u32[]{:S(2)}) copy-start(bf16[1,2048,1024]{2,1,0:T(8,128)(2,1)} %param.28) | copy-start | bytes 12582916
  98.3 6.3 %copy-start.9 = (u32[32]{0:T(128)S(1)}, u32[32]{0:T(128)}, u32[]{:S(2)}) copy-start(u32[32]{0:T(128)} %constant.133) | copy-start | bytes 388
  102.4 30.8 %collective-permute-start = (bf16[8,64,1024]{2,1,0:T(8,128)(2,1)S(1)}, bf16[8,64,1024]{2,1,0:T(8,128)(2,1)}, u32[]{:S(2)}, u32[]{:S(2)}) collective-permute-start(bf16[8,64,1024]{2,1,0:T(8,128)(2,1)S(1)} %multiply_convert_fusion), channel_id=1, source_target_pairs={{0,1},{1,2},{2,3},{3,0},{4,5},{5,6},{6,7},{7,4},{8,9},{9,10},{10,1... | collective-permute-start | bytes 3145736 | tf_op jit(solution)/shard_map/ppermute | solution.py:15
  131.8 58.8 %collective-permute-start.2 = (bf16[8,64,1024]{2,1,0:T(8,128)(2,1)S(1)}, bf16[8,64,1024]{2,1,0:T(8,128)(2,1)}, u32[]{:S(2)}, u32[]{:S(2)}) collective-permute-start(bf16[8,64,1024]{2,1,0:T(8,128)(2,1)S(1)} %multiply_convert_fusion), channel_id=1, source_target_pairs={{0,3},{1,0},{2,1},{3,2},{4,7},{5,4},{6,5},{7,6},{8,11},{9,8},{10,9... | collective-permute-start | bytes 3145736 | tf_op jit(solution)/shard_map/ppermute | solution.py:17
  133.2 54.6 %collective-permute-start.1 = (bf16[8,64,1024]{2,1,0:T(8,128)(2,1)}, bf16[8,64,1024]{2,1,0:T(8,128)(2,1)}, u32[]{:S(2)}, u32[]{:S(2)}) collective-permute-start(bf16[8,64,1024]{2,1,0:T(8,128)(2,1)} %collective-permute-done), channel_id=1, source_target_pairs={{0,1},{1,2},{2,3},{3,0},{4,5},{5,6},{6,7},{7,4},{8,9},{9,10},{10,1... | collective-permute-start | bytes 3145736 | tf_op jit(solution)/shard_map/ppermute | solution.py:15
  148.8 5.3 %copy-start.4 = (bf16[256,512]{1,0:T(8,128)(2,1)S(1)}, bf16[256,512]{1,0:T(8,128)(2,1)}, u32[]{:S(2)}) copy-start(bf16[256,512]{1,0:T(8,128)(2,1)} %param.20) | copy-start | bytes 786436
  191.9 4.3 %copy-start.8 = (bf16[1,4096,512]{2,1,0:T(8,128)(2,1)S(1)}, bf16[1,4096,512]{2,1,0:T(8,128)(2,1)}, u32[]{:S(2)}) copy-start(bf16[1,4096,512]{2,1,0:T(8,128)(2,1)} %param.29) | copy-start | bytes 12582916
  196.2 6.7 %copy-start.6 = (f32[256,2]{0,1:T(2,128)S(1)}, f32[256,2]{0,1:T(2,128)}, u32[]{:S(2)}) copy-start(f32[256,2]{0,1:T(2,128)} %param.26) | copy-start | bytes 6148
  199.4 18.8 %all-to-all-start.1 = ((bf16[8,64,512]{2,1,0:T(8,128)(2,1)}), bf16[8,64,512]{2,1,0:T(8,128)(2,1)S(1)}, u32[]{:S(2)}, u32[]{:S(2)}) async-start(bf16[8,64,512]{2,1,0:T(8,128)(2,1)} %fusion.15), calls=%async_computation.1 | async-start | bytes 1048576 | tf_op jit(solution)/shard_map/all_to_all | solution.py:151
Sparse Core Ops, SparseCore 0:
  44.4 48.1 all-gather.6
  156.2 31.9 all-gather.4
